TPU v7x, 32 devices: a whole 2x2x4 slice. The times are simulated.
32 devices in a mesh: sp: 8 (over z, y), tp: 4 (over x, core).
Axes of the slice: x: 2, y: 2, z: 4, core: 2. Of those that a mesh axis runs over, the one named last changes fastest.
Arguments:
- latent: bfloat16 [1024, 2048], P(('sp', 'tp')), may hold values from -6 to 6
- context: bfloat16 [512, 2048], replicated, may hold values from -6 to 6
- condition: float32 [2048], replicated, may hold values from -6 to 6
- context_condition: float32 [2048], replicated, may hold values from -6 to 6
- modulation_weight: bfloat16 [2048, 3, 2048], P('sp', None, 'tp'), may hold values from -0.25 to 0.25
- norm_gain: float32 [2048], replicated, may hold values from 0.1 to 1.9
- gate_weight: bfloat16 [2048, 1024], P(None, 'tp'), may hold values from -0.125 to 0.125
- value_weight: bfloat16 [2048, 1024], P(None, 'tp'), may hold values from -0.125 to 0.125
- write_weight: bfloat16 [2048, 512], P(None, 'tp'), may hold values from -0.125 to 0.125
- read_weight: bfloat16 [2048, 512], P(None, 'tp'), may hold values from -0.125 to 0.125
- step_weight: bfloat16 [2048, 2, 16], replicated, may hold values from -0.125 to 0.125
- value_taps: bfloat16 [3, 1024], P(None, 'tp'), may hold values from -3.5 to 3.5
- map_taps: bfloat16 [3, 2, 512], P(None, None, 'tp'), may hold values from -3.5 to 3.5
- decay_rate: float32 [2, 16], replicated, may hold values from 1e-06 to 0.06
- decay_jump: float32 [2, 16, 1024], P(None, 'tp', 'sp'), may hold values from -2.76 to 0
- skip_gain: float32 [16], replicated, may hold values from 1 to 16
- group_gain: float32 [1024], P('tp'), may hold values from 0.1 to 1.9
- output_weight: bfloat16 [1024, 2048], P('tp'), may hold values from -0.1875 to 0.1875
- post_gain: float32 [2048], replicated, may hold values from 0.1 to 1.9
Outputs:
- updated: bfloat16 [1024, 2048], P(('sp', 'tp'))
All inputs are finite; a program needn't handle non-finite values.
Results may differ from a plain program's by a relative error of at most 0.014.
Values may be sent and summed in bfloat16 or wider, within the bound.
A program may use at most 64 MiB of HBM per device.

v0:
```python
import jax
import jax.numpy as jnp
from jax import lax
from jax.sharding import PartitionSpec as P

HEAD_DIM = 64
STATE = 64
SPAN = 128
EPSILON = 1e-06
HIGHEST = lax.Precision.HIGHEST


def carried_in_2(shard, axis, combine, identity, reverse):
    size, mine = (lax.axis_size(axis), lax.axis_index(axis))
    everything = jax.tree.map(
        lambda part, kind: lax.all_gather(part.astype(kind), axis),
        shard,
        jax.tree.map(lambda a: jnp.bfloat16 if a.dtype == jnp.float32 else a.dtype, shard),
    )
    start = jax.tree.map(
        lambda part, zero: jnp.broadcast_to(jnp.asarray(zero, part.dtype), part.shape),
        shard,
        identity,
    )

    def turn(k, before):
        at = size - 1 - k if reverse else k
        reached = at > mine if reverse else at < mine
        new = combine(
            before, jax.tree.map(lambda part, own: part[at].astype(own.dtype), everything, shard)
        )
        return jax.tree.map(lambda a, b: jnp.where(reached, a, b), new, before)

    return lax.fori_loop(0, size, turn, start)


def with_halo(cells, sides, width):
    for axis, dim in sides:
        count = lax.axis_size(axis)
        ends = count - 1
        head = lax.slice_in_dim(cells, 0, width, axis=dim)
        tail = lax.slice_in_dim(cells, cells.shape[dim] - width, cells.shape[dim], axis=dim)
        cells = jnp.concatenate(
            [
                lax.ppermute(tail, axis, [(i, (i + 1) % count) for i in range(ends)]),
                cells,
                lax.ppermute(head, axis, [((i + 1) % count, i) for i in range(ends)]),
            ],
            axis=dim,
        )
    return cells


def modulated_norm(row_block, gain_vec, shift_vec, scale_vec):
    widened = row_block.astype(jnp.float32)
    normed = widened * lax.rsqrt(jnp.mean(widened * widened, axis=-1, keepdims=True) + EPSILON)
    return (normed * gain_vec * (1.0 + scale_vec) + shift_vec).astype(jnp.bfloat16)


def short_conv(padded, conv_taps):
    length = padded.shape[0] - 2
    widened = padded.astype(jnp.float32)
    weights = conv_taps.astype(jnp.float32)
    summed = (
        weights[0] * widened[:length]
        + weights[1] * widened[1 : length + 1]
        + weights[2] * widened[2:]
    )
    return jax.nn.silu(summed)


def zero_rim(tensor):
    return jnp.pad(tensor, ((1, 1), (0, 0)))


def project(row_block, weight):
    return jnp.dot(row_block, weight, preferred_element_type=jnp.float32).astype(jnp.bfloat16)


def flip_rows(tensor, direction):
    if direction == 1:
        return jnp.flip(tensor, axis=0)
    return tensor


def sweep(inputs, step_sizes, log_decay, write_maps, read_maps, start_state):
    length, head_count, head_width = inputs.shape
    blocks = length // SPAN
    lower_mask = (jnp.arange(SPAN)[:, None] >= jnp.arange(SPAN)[None, :])[:, :, None]

    def cut_blocks(tensor):
        return tensor.reshape((blocks, SPAN) + tensor.shape[1:])

    def advance(carry_state, block_data):
        value_block, size_block, decay_block, write_block, read_block = block_data
        within = jnp.cumsum(decay_block, axis=0)
        weighted = value_block * size_block[:, :, None]
        log_gaps = jnp.where(lower_mask, within[:, None, :] - within[None, :, :], 0.0)
        fading = jnp.where(lower_mask, jnp.exp(log_gaps), 0.0)
        scores = jnp.einsum("ihn,jhn->ijh", read_block, write_block, precision=HIGHEST) * fading
        inner_term = jnp.einsum("ijh,jhp->ihp", scores, weighted, precision=HIGHEST)
        carried = jnp.einsum(
            "ihn,hpn->ihp", read_block * jnp.exp(within)[:, :, None], carry_state, precision=HIGHEST
        )
        block_total = within[-1]
        fresh_state = jnp.einsum(
            "jhn,jhp->hpn",
            write_block * jnp.exp(block_total[None, :] - within)[:, :, None],
            weighted,
            precision=HIGHEST,
        )
        return (
            jnp.exp(block_total)[:, None, None] * carry_state + fresh_state,
            inner_term + carried,
        )

    final_state, outputs = lax.scan(
        advance,
        start_state,
        (
            cut_blocks(inputs),
            cut_blocks(step_sizes),
            cut_blocks(log_decay),
            cut_blocks(write_maps),
            cut_blocks(read_maps),
        ),
    )
    return (outputs.reshape(length, head_count, head_width), final_state)


def chain_join(earlier, later):
    return (earlier[0] + later[0], jnp.exp(later[0])[:, None, None] * earlier[1] + later[1])


def carried_in(direction, element, identity):
    if direction == 0:
        return carried_in_2(element, "sp", chain_join, identity, False)
    return carried_in_2(element, "sp", chain_join, identity, True)


def body(
    latent,
    context,
    condition,
    context_condition,
    modulation_weight,
    norm_gain,
    gate_weight,
    value_weight,
    write_weight,
    read_weight,
    step_weight,
    value_taps,
    map_taps,
    decay_rate,
    decay_jump,
    skip_gain,
    group_gain,
    output_weight,
    post_gain,
):
    head_devices = lax.axis_size("tp")
    head_rank = lax.axis_index("tp")
    token_rank = lax.axis_index("sp")
    model_width = norm_gain.shape[0]
    own_rows = modulation_weight.shape[0]
    head_local = value_weight.shape[1] // HEAD_DIM
    group_local = write_weight.shape[1] // STATE
    conditions = jax.nn.silu(jnp.stack([condition, context_condition]))
    own_conditions = lax.dynamic_slice_in_dim(conditions, token_rank * own_rows, own_rows, 1)
    partial_value = jnp.einsum(
        "sd,dkc->skc", own_conditions, modulation_weight.astype(jnp.float32), precision=HIGHEST
    )
    column_share = partial_value.shape[2]
    placed = jnp.zeros((2, 3, head_devices, column_share), jnp.float32)
    placed = lax.dynamic_update_slice(placed, partial_value[:, :, None, :], (0, 0, head_rank, 0))
    modulation = lax.psum(placed, ("sp", "tp")).reshape(2, 3, model_width)
    head_start = head_rank * head_local
    rate_local = lax.dynamic_slice_in_dim(decay_rate, head_start, head_local, 1)
    skip_local = lax.dynamic_slice_in_dim(skip_gain, head_start, head_local, 0)
    own_step = lax.dynamic_slice_in_dim(step_weight, head_start, head_local, 2).reshape(
        model_width, 2 * head_local
    )
    normed = modulated_norm(latent, norm_gain, modulation[0, 0], modulation[0, 1])
    gathered = lax.all_gather(normed, "tp", axis=0, tiled=True)
    token_count = gathered.shape[0]
    gate_linear = project(gathered, gate_weight)
    step_linear = project(gathered, own_step).reshape(token_count, 2, head_local)
    joined = jnp.concatenate(
        [
            project(gathered, value_weight),
            project(gathered, write_weight),
            project(gathered, read_weight),
        ],
        axis=1,
    )
    padded = with_halo(joined, (("sp", 0),), 1)
    conv_taps = jnp.concatenate([value_taps, map_taps.reshape(3, -1)], axis=1)
    convolved = short_conv(padded, conv_taps)
    value_width = head_local * HEAD_DIM
    map_width = group_local * STATE
    repeat_count = head_local // group_local
    latent_values = convolved[:, :value_width].reshape(token_count, head_local, HEAD_DIM)
    latent_write = jnp.repeat(
        convolved[:, value_width : value_width + map_width].reshape(
            token_count, group_local, STATE
        ),
        repeat_count,
        axis=1,
    )
    latent_read = jnp.repeat(
        convolved[:, value_width + map_width :].reshape(token_count, group_local, STATE),
        repeat_count,
        axis=1,
    )
    normed_context = modulated_norm(context, norm_gain, modulation[1, 0], modulation[1, 1])
    context_value = project(normed_context, value_weight)
    context_map = project(normed_context, write_weight)
    context_step = project(normed_context, own_step)
    context_length = context_value.shape[0]
    context_values = short_conv(zero_rim(context_value), value_taps).reshape(
        context_length, head_local, HEAD_DIM
    )
    context_write = short_conv(zero_rim(context_map), map_taps[:, 0]).reshape(
        context_length, group_local, STATE
    )
    context_write = jnp.repeat(context_write, repeat_count, axis=1)
    context_step = context_step.reshape(context_length, 2, head_local)
    mixer_sum = skip_local[None, :, None] * latent_values
    identity = (
        jnp.zeros((head_local,), jnp.float32),
        jnp.zeros((head_local, HEAD_DIM, STATE), jnp.float32),
    )
    for direction in range(2):
        rate_head = rate_local[direction]
        latent_size = jax.nn.softplus(step_linear[:, direction].astype(jnp.float32))
        latent_decay = -latent_size * rate_head[None, :] + decay_jump[direction].T
        context_size = jax.nn.softplus(context_step[:, direction].astype(jnp.float32))
        context_decay = -context_size * rate_head[None, :]
        unused_rows, context_state = sweep(
            flip_rows(context_values, direction),
            flip_rows(context_size, direction),
            flip_rows(context_decay, direction),
            flip_rows(context_write, direction),
            flip_rows(context_write, direction),
            identity[1],
        )
        oriented_decay = flip_rows(latent_decay, direction)
        swept_rows, local_state = sweep(
            flip_rows(latent_values, direction),
            flip_rows(latent_size, direction),
            oriented_decay,
            flip_rows(latent_write, direction),
            flip_rows(latent_read, direction),
            identity[1],
        )
        cumulative = jnp.cumsum(oriented_decay, axis=0)
        before_log, before_state = carried_in(direction, (cumulative[-1], local_state), identity)
        entering = before_state + jnp.exp(before_log)[:, None, None] * context_state
        carried = jnp.einsum(
            "ihn,hpn->ihp",
            flip_rows(latent_read, direction) * jnp.exp(cumulative)[:, :, None],
            entering,
            precision=HIGHEST,
        )
        mixer_sum = mixer_sum + flip_rows(swept_rows + carried, direction)
    gated_rows = mixer_sum.reshape(token_count, value_width) * jax.nn.silu(
        gate_linear.astype(jnp.float32)
    )
    grouped = gated_rows.reshape(token_count, group_local, value_width // group_local)
    grouped = (
        grouped
        * lax.rsqrt(jnp.mean(grouped * grouped, axis=-1, keepdims=True) + EPSILON)
        * group_gain.reshape(group_local, value_width // group_local)
    )
    gated_rows = grouped.reshape(token_count, value_width).astype(jnp.bfloat16)
    mixed_rows = lax.psum_scatter(
        jnp.dot(gated_rows, output_weight, preferred_element_type=jnp.float32).astype(jnp.bfloat16),
        "tp",
        scatter_dimension=0,
        tiled=True,
    ).astype(jnp.float32)
    normed_out = (
        mixed_rows
        * lax.rsqrt(jnp.mean(mixed_rows * mixed_rows, axis=-1, keepdims=True) + EPSILON)
        * post_gain
    )
    return (latent.astype(jnp.float32) + modulation[0, 2] * normed_out).astype(jnp.bfloat16)


def solution(mesh):
    placed = (
        P(("sp", "tp"), None),
        P(),
        P(),
        P(),
        P("sp", None, "tp"),
        P(),
        P(None, "tp"),
        P(None, "tp"),
        P(None, "tp"),
        P(None, "tp"),
        P(),
        P(None, "tp"),
        P(None, None, "tp"),
        P(),
        P(None, "tp", "sp"),
        P(),
        P("tp"),
        P("tp", None),
        P(),
    )
    return jax.shard_map(
        body, mesh=mesh, in_specs=placed, out_specs=P(("sp", "tp"), None), check_vma=False
    )
```

profile of v0, /device:TPU:0, one launch (start us, length us, event | category | flops | bytes accessed | tf_op | source)
XLA Modules:
  0.0 261.5 jit_solution(11595066028982531883)
XLA Ops:
  6.5 1.8 convolution_bitcast_fusion.2
  8.5 42.4 %psum.7 = f32[2,3,2048]{2,0,1:T(2,128)S(1)} all-reduce(f32[2,3,2048]{2,0,1:T(2,128)S(1)} %reshape.310), channel_id=1, replica_groups=mesh['sp'=8,'tp'=4] {'sp','tp'}, use_global_device_ids=true, to_apply=%region_0.1 | all-reduce | flops 12288 | bytes 98304 | tf_op jit(solution)/shard_map/psum | solution.py:177
  53.7 7.9 %all_gather.23 = bf16[128,2048]{1,0:T(8,128)(2,1)S(1)} all-gather(bf16[32,2048]{1,0:T(8,128)(2,1)S(1)} %fusion.38), channel_id=1, replica_groups=mesh['sp'=8,'tp'=4] {'tp'}, dimensions={0}, use_global_device_ids=true | all-gather | bytes 655360 | tf_op jit(solution)/shard_map/all_gather | solution.py:185
  63.1 3.4 %collective-permute-start = (bf16[1,512]{1,0:T(2,128)(2,1)}, bf16[1,512]{1,0:T(2,128)(2,1)}, u32[]{:S(2)}, u32[]{:S(2)}) collective-permute-start(bf16[1,512]{1,0:T(2,128)(2,1)} %get-tuple-element.648), channel_id=1, source_target_pairs={{0,4},{4,8},{8,12},{12,16},{16,20},{20,24},{24,28},{1,5},{5,9},{9,... | collective-permute-start | bytes 3080 | tf_op jit(solution)/shard_map/ppermute | solution.py:45
  67.8 2.2 fusion.13
  70.9 1.4 convolution_convert_fusion.1
  72.3 1.4 convolution_convert_fusion.2
  74.7 2.2 convolution_convert_fusion.7
  88.5 7.4 %while.67 = (s32[]{:T(128)}, f32[4,64,64]{2,1,0:T(8,128)S(1)}, f32[4,128,4]{1,2,0:T(4,128)S(1)}, f32[4,128,4,64]{1,3,2,0:T(8,128)}, f32[4,128,4]{1,2,0:T(4,128)S...) while((s32[]{:T(128)}, f32[4,64,64]{2,1,0:T(8,128)S(1)}, ...), condition=%wide.region_8.9_spmd.clone, body=%wide.region_6.8_spmd.clone.sunk | while | flops 25346052 | bytes 684759 | solution.py:117
  97.8 1.6 rev.42
  99.4 3.4 %rev.41 = f32[512,4,64]{0,2,1:T(8,128)} reverse(f32[512,4,64]{0,2,1:T(8,128)} %bitcast.243), dimensions={0} | reverse | bytes 1048576 | tf_op jit(solution)/shard_map/jit(_flip)/rev | solution.py:82
  104.0 1.7 rev.43
  105.7 2.0 reshape.324
  107.7 8.1 %while.69 = (s32[]{:T(128)}, f32[4,64,64]{2,1,0:T(8,128)S(1)}, f32[4,128,4]{2,1,0:T(8,128)S(1)}, f32[4,128,4,64]{1,0,3,2:T(4,128)S(1)}, f32[4,128,4]{1,2,0:T(4,1...) while((s32[]{:T(128)}, f32[4,64,64]{2,1,0:T(8,128)S(1)}, ...), condition=%wide.region_14.15_spmd.clone, body=%wide.region_12.14_spmd.clone.sunk | while | flops 25346052 | bytes 942295 | solution.py:117
  108.0 1.3 constant_dynamic-slice_fusion.13
  110.1 1.3 constant_dynamic-slice_fusion.13
  112.1 1.3 constant_dynamic-slice_fusion.13
  116.6 20.7 %all-gather.2 = bf16[8,1,4]{2,1,0:T(2,128)(2,1)S(1)} all-gather(bf16[1,1,4]{2,1,0:T(2,128)(2,1)} %convert_bitcast_fusion.1), channel_id=1, replica_groups=mesh['sp'=8,'tp'=4] {'sp'}, dimensions={0}, use_global_device_ids=true | all-gather | bytes 72 | tf_op jit(solution)/shard_map/all_gather | solution.py:16
  137.2 16.4 %all-gather.3 = bf16[8,1,4]{2,1,0:T(2,128)(2,1)S(1)} all-gather(bf16[1,1,4]{2,1,0:T(2,128)(2,1)} %convert_bitcast_fusion), channel_id=1, replica_groups=mesh['sp'=8,'tp'=4] {'sp'}, dimensions={0}, use_global_device_ids=true | all-gather | bytes 72 | tf_op jit(solution)/shard_map/all_gather | solution.py:16
  159.2 31.2 %all-gather = bf16[32,64,64]{2,1,0:T(8,128)(2,1)S(1)} all-gather(bf16[4,64,64]{2,1,0:T(8,128)(2,1)S(1)} %fusion.26), channel_id=2, replica_groups=mesh['sp'=8,'tp'=4] {'sp'}, dimensions={0}, use_global_device_ids=true | all-gather | bytes 294912 | tf_op jit(solution)/shard_map/all_gather | solution.py:16
  192.0 31.7 %all-gather.1 = bf16[32,64,64]{2,1,0:T(8,128)(2,1)S(1)} all-gather(bf16[4,64,64]{2,1,0:T(8,128)(2,1)S(1)} %fusion.27), channel_id=3, replica_groups=mesh['sp'=8,'tp'=4] {'sp'}, dimensions={0}, use_global_device_ids=true | all-gather | bytes 294912 | tf_op jit(solution)/shard_map/all_gather | solution.py:16
  228.4 1.6 fusion.113
  231.6 20.2 %reduce-scatter.2.cloned.1.call-done = bf16[32,2048]{1,0:T(8,128)(2,1)} async-done(((bf16[128,2048]{1,0:T(8,128)(2,1)}), bf16[32,2048]{1,0:T(8,128)(2,1)}) %reduce-scatter.2.cloned.1.call-update) | async-done | bytes 131088 | tf_op jit(solution)/shard_map/reduce_scatter | solution.py:277
  252.9 1.7 fusion.39
  (282 shorter events, 49.7 us)
Async XLA Ops:
  6.5 223.9 %copy-start = (bf16[256,2048]{1,0:T(8,128)(2,1)S(1)}, bf16[256,2048]{1,0:T(8,128)(2,1)}, u32[]{:S(2)}) copy-start(bf16[256,2048]{1,0:T(8,128)(2,1)} %param.44) | copy-start | bytes 3145732
  6.5 55.0 %copy-start.5 = (bf16[2048,256]{1,0:T(8,128)(2,1)S(1)}, bf16[2048,256]{1,0:T(8,128)(2,1)}, u32[]{:S(2)}) copy-start(bf16[2048,256]{1,0:T(8,128)(2,1)} %param.34) | copy-start | bytes 3145732
  6.5 245.3 %reduce-scatter.2.cloned.1.call-start = ((), (), s32[]{:S(2)}) async-start(), calls=%async_computation.1 | async-start | bytes 655360 | tf_op jit(solution)/shard_map/reduce_scatter | solution.py:277
  8.3 53.9 %copy-start.3 = (bf16[2048,128]{1,0:T(8,128)(2,1)S(1)}, bf16[2048,128]{1,0:T(8,128)(2,1)}, u32[]{:S(2)}) copy-start(bf16[2048,128]{1,0:T(8,128)(2,1)} %param.35) | copy-start | bytes 1572868
  50.9 10.9 %copy-start.8 = (bf16[2048,128]{1,0:T(8,128)(2,1)S(1)}, bf16[2048,128]{1,0:T(8,128)(2,1)}, u32[]{:S(2)}) copy-start(bf16[2048,128]{1,0:T(8,128)(2,1)} %param.36) | copy-start | bytes 1572868
  61.9 8.1 %copy-start.16 = (f32[2048]{0:T(1024)S(1)}, f32[2048]{0:T(1024)}, u32[]{:S(2)}) copy-start(f32[2048]{0:T(1024)} %param.32) | copy-start | bytes 24580
  62.2 8.7 %copy-start.9 = (bf16[128,128]{1,0:T(8,128)(2,1)}, bf16[128,128]{1,0:T(8,128)(2,1)S(1)}, u32[]{:S(2)}) copy-start(bf16[128,128]{1,0:T(8,128)(2,1)S(1)} %convolution_convert_fusion.5) | copy-start | bytes 98308
  62.5 8.4 %copy-start.11 = (bf16[128,128]{1,0:T(8,128)(2,1)}, bf16[128,128]{1,0:T(8,128)(2,1)S(1)}, u32[]{:S(2)}) copy-start(bf16[128,128]{1,0:T(8,128)(2,1)S(1)} %convolution_convert_fusion.6) | copy-start | bytes 98308
  63.1 93.7 %collective-permute-start = (bf16[1,512]{1,0:T(2,128)(2,1)}, bf16[1,512]{1,0:T(2,128)(2,1)}, u32[]{:S(2)}, u32[]{:S(2)}) collective-permute-start(bf16[1,512]{1,0:T(2,128)(2,1)} %get-tuple-element.648), channel_id=1, source_target_pairs={{0,4},{4,8},{8,12},{12,16},{16,20},{20,24},{24,28},{1,5},{5,9},{9,... | collective-permute-start | bytes 3080 | tf_op jit(solution)/shard_map/ppermute | solution.py:45
  66.5 90.4 %collective-permute-start.1 = (bf16[1,512]{1,0:T(2,128)(2,1)}, bf16[1,512]{1,0:T(2,128)(2,1)}, u32[]{:S(2)}, u32[]{:S(2)}) collective-permute-start(bf16[1,512]{1,0:T(2,128)(2,1)} %get-tuple-element.649), channel_id=1, source_target_pairs={{4,0},{8,4},{12,8},{16,12},{20,16},{24,20},{28,24},{5,1},{9,5},{13... | collective-permute-start | bytes 3080 | tf_op jit(solution)/shard_map/ppermute | solution.py:47
  88.5 8.2 %copy-start.25 = (bf16[3,2,128]{2,1,0:T(2,128)(2,1)S(1)}, bf16[3,2,128]{2,1,0:T(2,128)(2,1)}, u32[]{:S(2)}) copy-start(bf16[3,2,128]{2,1,0:T(2,128)(2,1)} %param.39) | copy-start | bytes 4612
  88.5 8.2 %copy-start.22 = (bf16[3,256]{1,0:T(4,128)(2,1)S(1)}, bf16[3,256]{1,0:T(4,128)(2,1)}, u32[]{:S(2)}) copy-start(bf16[3,256]{1,0:T(4,128)(2,1)} %param.38) | copy-start | bytes 4612
  88.5 8.7 %copy-start.18 = (f32[512,4]{0,1:T(4,128)S(1)}, f32[512,4]{0,1:T(4,128)}, u32[]{:S(2)}) copy-start(f32[512,4]{0,1:T(4,128)} %get-tuple-element.662) | copy-start | bytes 24580
  107.7 47.2 %copy-start.14 = (f32[128,4]{1,0:T(8,128)S(1)}, f32[128,4]{1,0:T(8,128)}, u32[]{:S(2)}) copy-start(f32[128,4]{1,0:T(8,128)} %get-tuple-element.650) | copy-start | bytes 6148
  107.7 49.1 %copy-start.10 = (bf16[128,128]{1,0:T(8,128)(2,1)S(1)}, bf16[128,128]{1,0:T(8,128)(2,1)}, u32[]{:S(2)}) copy-start(bf16[128,128]{1,0:T(8,128)(2,1)} %copy-done.9) | copy-start | bytes 98308
  107.7 49.1 %copy-start.12 = (bf16[128,128]{1,0:T(8,128)(2,1)S(1)}, bf16[128,128]{1,0:T(8,128)(2,1)}, u32[]{:S(2)}) copy-start(bf16[128,128]{1,0:T(8,128)(2,1)} %copy-done.11) | copy-start | bytes 98308
  115.8 43.0 %copy-start.19 = (f32[128,4]{0,1:T(4,128)S(1)}, f32[128,4]{0,1:T(4,128)}, u32[]{:S(2)}) copy-start(f32[128,4]{0,1:T(4,128)} %get-tuple-element.668) | copy-start | bytes 6148
  115.9 43.0 %copy-start.30 = (f32[4]{0:T(128)S(1)}, f32[4]{0:T(128)}, u32[]{:S(2)}) copy-start(f32[4]{0:T(128)} %exponential_multiply_fusion.1) | copy-start | bytes 52
  155.0 35.5 %copy-start.20 = (f32[4]{0:T(128)S(1)}, f32[4]{0:T(128)}, u32[]{:S(2)}) copy-start(f32[4]{0:T(128)} %custom-call) | copy-start | bytes 52
  158.4 33.2 %copy-start.29 = (f32[4]{0:T(128)S(1)}, f32[4]{0:T(128)}, u32[]{:S(2)}) copy-start(f32[4]{0:T(128)} %exponential_multiply_fusion) | copy-start | bytes 52
  191.5 33.7 %copy-start.15 = (pred[128,128]{0,1:T(8,128)(4,1)S(1)}, pred[128,128]{0,1:T(8,128)(4,1)}, u32[]{:S(2)}) copy-start(pred[128,128]{0,1:T(8,128)(4,1)} %iota_compare_fusion) | copy-start | bytes 49156
  229.9 23.0 %copy-start.4 = (bf16[32,2048]{1,0:T(8,128)(2,1)S(1)}, bf16[32,2048]{1,0:T(8,128)(2,1)}, u32[]{:S(2)}) copy-start(bf16[32,2048]{1,0:T(8,128)(2,1)} %param.27) | copy-start | bytes 393220
  229.9 23.0 %copy-start.17 = (f32[1,1,2048]{2,0,1:T(1,128)S(1)}, f32[1,1,2048]{2,0,1:T(1,128)}, u32[]{:S(2)}) copy-start(f32[1,1,2048]{2,0,1:T(1,128)} %get-tuple-element.654) | copy-start | bytes 24580
  229.9 23.0 %copy-start.23 = (f32[2048]{0:T(1024)S(1)}, f32[2048]{0:T(1024)}, u32[]{:S(2)}) copy-start(f32[2048]{0:T(1024)} %param.45) | copy-start | bytes 24580
  (11 other events, 49.4 us)
Sparse Core Ops, SparseCore 0:
  231.8 20.0 reduce-scatter.1
where the time goes:
time: 263 us; the launch traced here: 261 us
  blocking collectives  150 us (57%)
  local copies, waits for them, and re-layouts  29.5 us (11%)
  other arithmetic  20.9 us (8%)
  matrix products  20.8 us (8%)
  waiting for transfers between devices  20.2 us (8%)
  between operations  14.2 us (5%)
  starting transfers between devices  4.64 us (2%)
    all_gather x4, blocking collectives, carried_in_2(): lax.all_gather(part.astype(kind), axis)  100 us
    psum x1, blocking collectives, body(): modulation = lax.psum(placed, ('sp', 'tp')).reshape(2, 3, model_width)  42.4 us
    reduce_scatter x1, waiting for transfers between devices, body(): lax.psum_scatter(jnp.dot(gated_rows, output_weight, preferred_element_typ...  20.2 us
    rev x12, local copies, waits for them, and re-layouts, flip_rows(): return jnp.flip(tensor, axis=0)  9.24 us
    all_gather x1, blocking collectives, body(): gathered = lax.all_gather(normed, 'tp', axis=0, tiled=True)  7.89 us
    dot_general x8, matrix products, project(): jnp.dot(row_block, weight, preferred_element_type=jnp.float32)  7.73 us
    dot_general x10, matrix products, advance(): jnp.einsum('jhn,jhp->hpn', write_block * jnp.exp(block_total[None, :] - w...  7.06 us
    dynamic_slice x16, local copies, waits for them, and re-layouts, sweep(): lax.scan(advance, start_state, (cut_blocks(inputs), cut_blocks(step_sizes...  6.44 us
  transfers between devices with their start and end apart: 3, of which 1 were waited for; matrix products, arithmetic and copies ran while one was open for 20% of the time, Pallas kernels for 0%

commit v1 on v0

--- a/solution.py
+++ b/solution.py
@@ -174,7 +174,7 @@
     column_share = partial_value.shape[2]
     placed = jnp.zeros((2, 3, head_devices, column_share), jnp.float32)
     placed = lax.dynamic_update_slice(placed, partial_value[:, :, None, :], (0, 0, head_rank, 0))
-    modulation = lax.psum(placed, ("sp", "tp")).reshape(2, 3, model_width)
+    modulation = jnp.sum(lax.all_gather(placed, ("sp", "tp")), axis=0).reshape(2, 3, model_width)
     head_start = head_rank * head_local
     rate_local = lax.dynamic_slice_in_dim(decay_rate, head_start, head_local, 1)
     skip_local = lax.dynamic_slice_in_dim(skip_gain, head_start, head_local, 0)

time: 263 us -> 298 us (1.13)
  waiting for transfers between devices: 20.2 us -> 65.8 us
  blocking collectives: 150 us -> 107 us
  other arithmetic: 20.9 us -> 40.7 us
  local copies, waits for them, and re-layouts: 29.5 us -> 40.6 us
    all_gather x0 -> x1, waiting for transfers between devices: none -> 46.1 us  [body(): lax.all_gather(placed, ('sp', 'tp'))]
    psum x1 -> x0, blocking collectives: 42.4 us -> none  [body(): modulation = lax.psum(placed, ('sp', 'tp')).reshape(2, 3, model_width)]
    exp x16, other arithmetic: 0.28 us -> 15.4 us  [chain_join(): jnp.exp(later[0])[:, None, None] * earlier[1] + later[1]]
    unnamed x70 -> x92, local copies, waits for them, and re-layouts: 2.66 us -> 5.74 us
  transfers between devices with their start and end apart: 3 -> 4, of which waited for: 1 -> 2; matrix products, arithmetic and copies ran while one was open for 20% -> 12% of each run, Pallas kernels for 0% -> 0%
where the time goes in v1:
time: 298 us; the launch traced here: 296 us
  blocking collectives  107 us (36%)
  waiting for transfers between devices  65.8 us (22%)
  other arithmetic  40.7 us (14%)
  local copies, waits for them, and re-layouts  40.6 us (14%)
  matrix products  22.1 us (7%)
  between operations  14.3 us (5%)
  starting transfers between devices  5.27 us (2%)
    all_gather x4, blocking collectives, carried_in_2(): lax.all_gather(part.astype(kind), axis)  99.3 us
    all_gather x1, waiting for transfers between devices, body(): lax.all_gather(placed, ('sp', 'tp'))  46.1 us
    reduce_scatter x1, waiting for transfers between devices, body(): lax.psum_scatter(jnp.dot(gated_rows, output_weight, preferred_element_typ...  19.7 us
    exp x16, other arithmetic, chain_join(): jnp.exp(later[0])[:, None, None] * earlier[1] + later[1]  15.4 us
    rev x12, local copies, waits for them, and re-layouts, flip_rows(): return jnp.flip(tensor, axis=0)  9.79 us
    dot_general x8, matrix products, project(): jnp.dot(row_block, weight, preferred_element_type=jnp.float32)  8.39 us
    dot_general x10, matrix products, advance(): jnp.einsum('jhn,jhp->hpn', write_block * jnp.exp(block_total[None, :] - w...  7.74 us
    all_gather x1, blocking collectives, body(): gathered = lax.all_gather(normed, 'tp', axis=0, tiled=True)  7.29 us
  transfers between devices with their start and end apart: 4, of which 2 were waited for; matrix products, arithmetic and copies ran while one was open for 12% of the time, Pallas kernels for 0%

profile of v1, /device:TPU:0, one launch (start us, length us, event | category | flops | bytes accessed | tf_op | source)
XLA Modules:
  0.0 296.4 jit_solution(13662566286590226844)
XLA Ops:
  6.5 1.7 convolution_bitcast_fusion.2
  19.0 2.1 fusion.13
  21.7 46.1 %all-gather.6.cloned.1.call-done = f32[32,2,3,4,512]{4,3,2,1,0:T(4,128)} async-done(((f32[1,2,3,4,512]{4,3,2,1,0:T(4,128)}), f32[32,2,3,4,512]{4,3,2,1,0:T(4,128)}) %all-gather.6.cloned.1.call-update) | async-done | bytes 1572880 | tf_op jit(solution)/shard_map/all_gather | solution.py:177
  67.8 2.3 reduce_sum.45
  71.5 1.5 reshape.313
  72.9 1.4 fusion.111
  76.5 1.4 convolution_convert_fusion.1
  78.0 7.3 %all_gather.31 = bf16[128,2048]{1,0:T(8,128)(2,1)S(1)} all-gather(bf16[32,2048]{1,0:T(8,128)(2,1)S(1)} %fusion.38), channel_id=1, replica_groups=mesh['sp'=8,'tp'=4] {'tp'}, dimensions={0}, use_global_device_ids=true | all-gather | bytes 655360 | tf_op jit(solution)/shard_map/all_gather | solution.py:185
  100.1 7.4 %while.67 = (s32[]{:T(128)}, f32[4,64,64]{2,1,0:T(8,128)S(1)}, f32[4,128,4]{1,2,0:T(4,128)S(1)}, f32[4,128,4,64]{1,3,2,0:T(8,128)}, f32[4,128,4]{1,2,0:T(4,128)S...) while((s32[]{:T(128)}, f32[4,64,64]{2,1,0:T(8,128)S(1)}, ...), condition=%wide.region_8.9_spmd.clone, body=%wide.region_6.8_spmd.clone.sunk | while | flops 25346052 | bytes 684759 | solution.py:117
  110.2 3.9 %collective-permute-start = (bf16[1,512]{1,0:T(2,128)(2,1)}, bf16[1,512]{1,0:T(2,128)(2,1)}, u32[]{:S(2)}, u32[]{:S(2)}) collective-permute-start(bf16[1,512]{1,0:T(2,128)(2,1)} %get-tuple-element.648), channel_id=1, source_target_pairs={{0,4},{4,8},{8,12},{12,16},{16,20},{20,24},{24,28},{1,5},{5,9},{9,... | collective-permute-start | bytes 3080 | tf_op jit(solution)/shard_map/ppermute | solution.py:45
  114.6 1.6 rev.42
  116.2 3.4 %rev.41 = f32[512,4,64]{0,2,1:T(8,128)} reverse(f32[512,4,64]{0,2,1:T(8,128)} %bitcast.243), dimensions={0} | reverse | bytes 1048576 | tf_op jit(solution)/shard_map/jit(_flip)/rev | solution.py:82
  120.8 1.7 rev.43
  122.5 2.0 reshape.327
  124.6 8.1 %while.69 = (s32[]{:T(128)}, f32[4,64,64]{2,1,0:T(8,128)S(1)}, f32[4,128,4]{2,1,0:T(8,128)S(1)}, f32[4,128,4,64]{1,0,3,2:T(4,128)S(1)}, f32[4,128,4]{1,2,0:T(4,1...) while((s32[]{:T(128)}, f32[4,64,64]{2,1,0:T(8,128)S(1)}, ...), condition=%wide.region_14.15_spmd.clone, body=%wide.region_12.14_spmd.clone.sunk | while | flops 25346052 | bytes 942295 | solution.py:117
  134.6 20.1 %all-gather.2 = bf16[8,1,4]{2,1,0:T(2,128)(2,1)S(1)} all-gather(bf16[1,1,4]{2,1,0:T(2,128)(2,1)} %convert_bitcast_fusion.1), channel_id=1, replica_groups=mesh['sp'=8,'tp'=4] {'sp'}, dimensions={0}, use_global_device_ids=true | all-gather | bytes 72 | tf_op jit(solution)/shard_map/all_gather | solution.py:16
  154.8 16.4 %all-gather.3 = bf16[8,1,4]{2,1,0:T(2,128)(2,1)S(1)} all-gather(bf16[1,1,4]{2,1,0:T(2,128)(2,1)} %convert_bitcast_fusion), channel_id=1, replica_groups=mesh['sp'=8,'tp'=4] {'sp'}, dimensions={0}, use_global_device_ids=true | all-gather | bytes 72 | tf_op jit(solution)/shard_map/all_gather | solution.py:16
  178.4 31.2 %all-gather = bf16[32,64,64]{2,1,0:T(8,128)(2,1)S(1)} all-gather(bf16[4,64,64]{2,1,0:T(8,128)(2,1)S(1)} %fusion.26), channel_id=2, replica_groups=mesh['sp'=8,'tp'=4] {'sp'}, dimensions={0}, use_global_device_ids=true | all-gather | bytes 294912 | tf_op jit(solution)/shard_map/all_gather | solution.py:16
  209.6 10.7 %while.66 = (s32[]{:T(128)}, f32[4]{0:T(128)}, f32[4,64,64]{2,1,0:T(8,128)S(1)}, s32[]{:T(128)}, bf16[8,4]{1,0:T(8,128)(2,1)}, /*index=5*/bf16[8,4,64,64]{3,2,1,0:T(8,128)(2,1)S(1)}, s32[]{:T(128)}, s32[]{:T(128)}) while((s32[]{:T(128)}, f32[4]{0:T(128)}, f32[4,64,64]{2,1,0:T(8,128)S(1)}, s32[]{:T(128)}, bf16[8,4]{1,0:T(8,128)(2,1)}, ...), condition=%wide.region_4.5_spmd.clone, body=%wide.region_3.4_spmd.clone.sunk | while | flops 81940 | bytes 164027 | solution.py:34
  222.1 31.6 %all-gather.1 = bf16[32,64,64]{2,1,0:T(8,128)(2,1)S(1)} all-gather(bf16[4,64,64]{2,1,0:T(8,128)(2,1)S(1)} %fusion.27), channel_id=3, replica_groups=mesh['sp'=8,'tp'=4] {'sp'}, dimensions={0}, use_global_device_ids=true | all-gather | bytes 294912 | tf_op jit(solution)/shard_map/all_gather | solution.py:16
  253.7 6.5 %while.68 = (s32[]{:T(128)}, f32[4]{0:T(128)S(1)}, f32[4,64,64]{2,1,0:T(8,128)S(1)}, s32[]{:T(128)}, bf16[8,4]{1,0:T(8,128)(2,1)}, /*index=5*/bf16[8,4,64,64]{3,...) while((s32[]{:T(128)}, f32[4]{0:T(128)S(1)}, f32[4,64,64]{2,1,0:T(8,128)S(1)}, ...), condition=%wide.region_11.12_spmd.clone, body=%wide.region_10.11_spmd.clone.sunk | while | flops 81944 | bytes 164089 | solution.py:34
  263.8 1.6 fusion.113
  267.1 19.7 %reduce-scatter.2.cloned.1.call-done = bf16[32,2048]{1,0:T(8,128)(2,1)} async-done(((bf16[128,2048]{1,0:T(8,128)(2,1)}), bf16[32,2048]{1,0:T(8,128)(2,1)}) %reduce-scatter.2.cloned.1.call-update) | async-done | bytes 131088 | tf_op jit(solution)/shard_map/reduce_scatter | solution.py:277
  287.8 1.7 fusion.39
  (308 shorter events, 82.5 us)
Async XLA Ops:
  6.5 259.4 %copy-start = (bf16[256,2048]{1,0:T(8,128)(2,1)S(1)}, bf16[256,2048]{1,0:T(8,128)(2,1)}, u32[]{:S(2)}) copy-start(bf16[256,2048]{1,0:T(8,128)(2,1)} %param.44) | copy-start | bytes 3145732
  6.5 14.6 %copy-start.30 = (bf16[3,256]{1,0:T(4,128)(2,1)S(1)}, bf16[3,256]{1,0:T(4,128)(2,1)}, u32[]{:S(2)}) copy-start(bf16[3,256]{1,0:T(4,128)(2,1)} %param.38) | copy-start | bytes 4612
  6.5 61.2 %all-gather.6.cloned.1.call-start = ((), (), s32[]{:S(2)}) async-start(), calls=%async_computation.1 | async-start | bytes 1622016 | tf_op jit(solution)/shard_map/all_gather | solution.py:177
  9.1 277.7 %reduce-scatter.2.cloned.1.call-start = ((), (), s32[]{:S(2)}) async-start(), calls=%async_computation.2 | async-start | bytes 655360 | tf_op jit(solution)/shard_map/reduce_scatter | solution.py:277
  11.4 63.0 %copy-start.1 = (bf16[512,2048]{1,0:T(8,128)(2,1)S(1)}, bf16[512,2048]{1,0:T(8,128)(2,1)}, u32[]{:S(2)}) copy-start(bf16[512,2048]{1,0:T(8,128)(2,1)} %param.28) | copy-start | bytes 6291460
  11.4 63.0 %copy-start.23 = (f32[2048]{0:T(1024)S(1)}, f32[2048]{0:T(1024)}, u32[]{:S(2)}) copy-start(f32[2048]{0:T(1024)} %param.32) | copy-start | bytes 24580
  100.0 9.5 %copy-start.7 = (bf16[128,256]{1,0:T(8,128)(2,1)S(1)}, bf16[128,256]{1,0:T(8,128)(2,1)}, u32[]{:S(2)}) copy-start(bf16[128,256]{1,0:T(8,128)(2,1)} %convolution_convert_fusion.4) | copy-start | bytes 196612
  100.0 9.5 %copy-start.15 = (bf16[128,128]{1,0:T(8,128)(2,1)S(1)}, bf16[128,128]{1,0:T(8,128)(2,1)}, u32[]{:S(2)}) copy-start(bf16[128,128]{1,0:T(8,128)(2,1)} %convolution_convert_fusion.6) | copy-start | bytes 98308
  100.1 14.1 %copy-start.25 = (f32[512,4]{0,1:T(4,128)S(1)}, f32[512,4]{0,1:T(4,128)}, u32[]{:S(2)}) copy-start(f32[512,4]{0,1:T(4,128)} %get-tuple-element.662) | copy-start | bytes 24580
  110.2 65.8 %collective-permute-start = (bf16[1,512]{1,0:T(2,128)(2,1)}, bf16[1,512]{1,0:T(2,128)(2,1)}, u32[]{:S(2)}, u32[]{:S(2)}) collective-permute-start(bf16[1,512]{1,0:T(2,128)(2,1)} %get-tuple-element.648), channel_id=1, source_target_pairs={{0,4},{4,8},{8,12},{12,16},{16,20},{20,24},{24,28},{1,5},{5,9},{9,... | collective-permute-start | bytes 3080 | tf_op jit(solution)/shard_map/ppermute | solution.py:45
  124.5 46.7 %copy-start.11 = (f32[128,4]{1,0:T(8,128)S(1)}, f32[128,4]{1,0:T(8,128)}, u32[]{:S(2)}) copy-start(f32[128,4]{1,0:T(8,128)} %copy-done.9) | copy-start | bytes 6148
  124.5 48.5 %copy-start.20 = (f32[128,4]{1,0:T(8,128)S(1)}, f32[128,4]{1,0:T(8,128)}, u32[]{:S(2)}) copy-start(f32[128,4]{1,0:T(8,128)} %get-tuple-element.650) | copy-start | bytes 6148
  124.5 51.4 %copy-start.8 = (bf16[128,256]{1,0:T(8,128)(2,1)S(1)}, bf16[128,256]{1,0:T(8,128)(2,1)}, u32[]{:S(2)}) copy-start(bf16[128,256]{1,0:T(8,128)(2,1)} %convolution_convert_fusion.4) | copy-start | bytes 196612
  124.5 51.4 %copy-start.16 = (bf16[128,128]{1,0:T(8,128)(2,1)S(1)}, bf16[128,128]{1,0:T(8,128)(2,1)}, u32[]{:S(2)}) copy-start(bf16[128,128]{1,0:T(8,128)(2,1)} %convolution_convert_fusion.6) | copy-start | bytes 98308
  124.6 51.4 %copy-start.18 = (bf16[128,128]{1,0:T(8,128)(2,1)S(1)}, bf16[128,128]{1,0:T(8,128)(2,1)}, u32[]{:S(2)}) copy-start(bf16[128,128]{1,0:T(8,128)(2,1)} %copy-done.17) | copy-start | bytes 98308
  132.7 45.3 %copy-start.26 = (f32[128,4]{0,1:T(4,128)S(1)}, f32[128,4]{0,1:T(4,128)}, u32[]{:S(2)}) copy-start(f32[128,4]{0,1:T(4,128)} %get-tuple-element.668) | copy-start | bytes 6148
  132.7 45.3 %copy-start.40 = (f32[4]{0:T(128)S(1)}, f32[4]{0:T(128)}, u32[]{:S(2)}) copy-start(f32[4]{0:T(128)} %exponential_multiply_fusion.1) | copy-start | bytes 52
  133.3 42.7 %collective-permute-start.1 = (bf16[1,512]{1,0:T(2,128)(2,1)}, bf16[1,512]{1,0:T(2,128)(2,1)S(1)}, u32[]{:S(2)}, u32[]{:S(2)}) collective-permute-start(bf16[1,512]{1,0:T(2,128)(2,1)} %get-tuple-element.649), channel_id=1, source_target_pairs={{4,0},{8,4},{12,8},{16,12},{20,16},{24,20},{28,24},{5,1},{9,5},{13... | collective-permute-start | bytes 3080 | tf_op jit(solution)/shard_map/ppermute | solution.py:47
  177.9 75.8 %copy-start.29 = (f32[4]{0:T(128)S(1)}, f32[4]{0:T(128)}, u32[]{:S(2)}) copy-start(f32[4]{0:T(128)} %custom-call.3) | copy-start | bytes 52
  220.3 40.3 %copy-start.22 = (pred[128,128]{0,1:T(8,128)(4,1)S(1)}, pred[128,128]{0,1:T(8,128)(4,1)}, u32[]{:S(2)}) copy-start(pred[128,128]{0,1:T(8,128)(4,1)} %iota_compare_fusion) | copy-start | bytes 49156
  222.1 39.5 %copy-start.28 = (f32[128,4]{0,1:T(4,128)S(1)}, f32[128,4]{0,1:T(4,128)}, u32[]{:S(2)}) copy-start(f32[128,4]{0,1:T(4,128)} %rev.36) | copy-start | bytes 6148
  265.4 22.4 %copy-start.5 = (bf16[32,2048]{1,0:T(8,128)(2,1)S(1)}, bf16[32,2048]{1,0:T(8,128)(2,1)}, u32[]{:S(2)}) copy-start(bf16[32,2048]{1,0:T(8,128)(2,1)} %param.27) | copy-start | bytes 393220
  265.4 22.4 %copy-start.24 = (f32[1,1,2048]{2,0,1:T(1,128)S(1)}, f32[1,1,2048]{2,0,1:T(1,128)}, u32[]{:S(2)}) copy-start(f32[1,1,2048]{2,0,1:T(1,128)} %get-tuple-element.654) | copy-start | bytes 24580
  265.4 22.4 %copy-start.31 = (f32[2048]{0:T(1024)S(1)}, f32[2048]{0:T(1024)}, u32[]{:S(2)}) copy-start(f32[2048]{0:T(1024)} %param.45) | copy-start | bytes 24580
  (23 other events, 95.4 us)
Sparse Core Ops, SparseCore 0:
  10.2 57.5 all-gather.5
  267.2 19.5 reduce-scatter.1
